TPU v7x, 32 devices: a whole 2x2x4 slice. The times are simulated.
32 devices in a mesh: sp: 16 (over z, y, x), tp: 2 (over core).
Axes of the slice: x: 2, y: 2, z: 4, core: 2. Of those that a mesh axis runs over, the one named last changes fastest.
Arguments:
- residual: bfloat16 [6144, 2048], P('sp'), may hold values from -6 to 6
- queries: bfloat16 [6144, 2048], P('sp', 'tp'), may hold values from -48 to 48
- keys: bfloat16 [6144, 2048], P('sp', 'tp'), may hold values from -48 to 48
- values: bfloat16 [6144, 2048], P('sp', 'tp'), may hold values from -6 to 6
- gate_cache: float32 [6144, 32], P('sp', 'tp'), may hold values from -1544 to 0, as said below
- doc_ids: int32 [6144], P('sp'), may hold values from 0 to 7, never falling along the last dimension, each value on 1 to 1536 neighbouring positions
- out_weight: bfloat16 [2048, 2048], P('tp'), may hold values from -1 to 1
- mix_gain: float32 [2048], replicated, may hold values from 0.1 to 1.9
- gate_weight: bfloat16 [2048, 5120], P('sp', 'tp'), may hold values from -0.125 to 0.125
- up_weight: bfloat16 [2048, 5120], P('sp', 'tp'), may hold values from -0.125 to 0.125
- down_weight: bfloat16 [5120, 2048], P('tp', 'sp'), may hold values from -0.15625 to 0.15625
Outputs:
- layer_out: bfloat16 [6144, 2048], P(('sp', 'tp'))
Inputs may be any that keep to these rules, and one draw needn't show every extreme that they name: `doc_ids`: positions of one document are consecutive; each document has 1 to 1536 positions, and one has exactly that many. `gate_cache`: no column rises from one position to the next.
All inputs are finite; a program needn't handle non-finite values.
Results may differ from a plain program's by a relative error of at most 0.018.
Values may be sent and summed in bfloat16 or wider, within the bound.
No kernel may reach another device: no remote copies, remote signals or barrier semaphores. Data moves between devices by JAX's collectives and lax.ppermute only.
A program may use at most 128 MiB of HBM per device.

v0:
```python
import jax
import jax.numpy as jnp
from jax import lax
from jax.sharding import PartitionSpec as P

REACH = 4


EPSILON = 1e-06
NEGATIVE = -1e30


def from_behind(value, axis, steps):
    count = lax.axis_size(axis)
    first, last = (max(0, -steps), min(count, count - steps))
    return lax.ppermute(value, axis, [(source, source + steps) for source in range(first, last)])


def normalize(middle, gain):
    widened = middle.astype(jnp.float32)
    factor = lax.rsqrt(jnp.mean(widened * widened, axis=-1, keepdims=True) + EPSILON)
    return (widened * factor * gain).astype(jnp.bfloat16)


def local(
    residual,
    queries,
    keys,
    values,
    gate_cache,
    doc_ids,
    out_weight,
    mix_gain,
    gate_weight,
    up_weight,
    down_weight,
):
    tok_rows = queries.shape[0]
    heads_here = gate_cache.shape[1]
    head_size = queries.shape[1] // heads_here
    sp_index = lax.axis_index("sp")
    key_parts = [keys]
    value_parts = [values]
    cache_parts = [gate_cache]
    doc_parts = [doc_ids]
    for distance in range(1, REACH + 1):
        moved_keys, moved_values = from_behind((keys, values), "sp", distance)
        moved_cache, moved_docs = from_behind((gate_cache, doc_ids), "sp", distance)
        key_parts.append(moved_keys)
        value_parts.append(moved_values)
        cache_parts.append(moved_cache)
        doc_parts.append(moved_docs)
    all_keys = jnp.concatenate(key_parts[::-1], axis=0)
    all_values = jnp.concatenate(value_parts[::-1], axis=0)
    all_cache = jnp.concatenate(cache_parts[::-1], axis=0)
    all_docs = jnp.concatenate(doc_parts[::-1], axis=0)
    key_count = all_keys.shape[0]
    query_pos = sp_index * tok_rows + jnp.arange(tok_rows, dtype=jnp.int32)
    key_pos = (sp_index - REACH) * tok_rows + jnp.arange(key_count, dtype=jnp.int32)
    visible = (
        (key_pos[None, :] <= query_pos[:, None])
        & (key_pos[None, :] >= 0)
        & (all_docs[None, :] == doc_ids[:, None])
    )
    query_heads = queries.reshape(tok_rows, heads_here, head_size)
    key_heads = all_keys.reshape(key_count, heads_here, head_size)
    value_heads = all_values.reshape(key_count, heads_here, head_size)
    score_scale = head_size ** (-0.5)
    scores = (
        jnp.einsum("qhd,khd->hqk", query_heads, key_heads, preferred_element_type=jnp.float32)
        * score_scale
    )
    scores = scores + gate_cache.T[:, :, None] - all_cache.T[:, None, :]
    scores = jnp.where(visible[None], scores, NEGATIVE)
    row_max = jnp.max(scores, axis=-1, keepdims=True)
    exp_scores = jnp.exp(scores - row_max)
    weights = (exp_scores / jnp.sum(exp_scores, axis=-1, keepdims=True)).astype(jnp.bfloat16)
    attended = jnp.einsum("hqk,khd->qhd", weights, value_heads, preferred_element_type=jnp.float32)
    attended = attended.astype(jnp.bfloat16).reshape(tok_rows, heads_here * head_size)
    row_share = tok_rows // lax.axis_size("tp")
    tp_index = lax.axis_index("tp")
    partial_value = jnp.dot(attended, out_weight, preferred_element_type=jnp.float32)
    attn_sum = lax.psum(partial_value.astype(jnp.bfloat16), "tp").astype(jnp.float32)
    whole_middle = (residual.astype(jnp.float32) + attn_sum).astype(jnp.bfloat16)
    mixer_in = normalize(whole_middle, mix_gain)
    middle = lax.dynamic_slice_in_dim(whole_middle, tp_index * row_share, row_share, 0)
    held_gate, held_up = (
        lax.all_gather(gate_weight, "sp", axis=0, tiled=True),
        lax.all_gather(up_weight, "sp", axis=0, tiled=True),
    )
    gate_proj = jnp.dot(mixer_in, held_gate, preferred_element_type=jnp.float32)
    up_proj = jnp.dot(mixer_in, held_up, preferred_element_type=jnp.float32)
    hidden = (jax.nn.silu(gate_proj) * up_proj).astype(jnp.bfloat16)
    partials = jnp.dot(
        hidden,
        lax.all_gather(down_weight, "sp", axis=1, tiled=True),
        preferred_element_type=jnp.float32,
    )
    down_sum = lax.psum_scatter(
        partials.astype(jnp.bfloat16), "tp", scatter_dimension=0, tiled=True
    ).astype(jnp.float32)
    return (middle.astype(jnp.float32) + down_sum).astype(jnp.bfloat16)


def solution(mesh):
    return jax.shard_map(
        local,
        mesh=mesh,
        in_specs=(
            P("sp", None),
            P("sp", "tp"),
            P("sp", "tp"),
            P("sp", "tp"),
            P("sp", "tp"),
            P("sp"),
            P("tp", None),
            P(),
            P("sp", "tp"),
            P("sp", "tp"),
            P("tp", "sp"),
        ),
        out_specs=P(("sp", "tp"), None),
        check_vma=False,
    )
```

profile of v0, /device:TPU:0, one launch (start us, length us, event | category | flops | bytes accessed | tf_op | source)
XLA Modules:
  0.0 706.5 jit_solution(17122347479193859977)
XLA Ops:
  7.4 5.1 collective-permute-start.4
  12.5 4.4 collective-permute-start.5
  16.8 3.4 collective-permute-start.6
  22.8 3.5 collective-permute-start.8
  27.9 3.9 collective-permute-start.9
  31.8 3.4 collective-permute-start.10
  39.1 3.2 compare_and_fusion
  42.7 54.6 %collective-permute-start.13 = (f32[384,16]{0,1:T(8,128)}, f32[384,16]{0,1:T(8,128)S(1)}, u32[]{:S(2)}, u32[]{:S(2)}) collective-permute-start(f32[384,16]{0,1:T(8,128)} %param.15), channel_id=1, source_target_pairs={{0,6},{2,8},{4,10},{6,12},{8,14},{10,16},{12,18},{14,20},{16,22},{... | collective-permute-start | bytes 73736 | tf_op jit(solution)/shard_map/ppermute | solution.py:16
  102.0 6.3 collective-permute-start.15
  110.0 8.2 %collective-permute-start = (bf16[384,1024]{1,0:T(8,128)(2,1)}, bf16[384,1024]{1,0:T(8,128)(2,1)S(1)}, u32[]{:S(2)}, u32[]{:S(2)}) collective-permute-start(bf16[384,1024]{1,0:T(8,128)(2,1)} %param.14), channel_id=1, source_target_pairs={{0,8},{2,10},{4,12},{6,14},{8,16},{10,18},{12,20},{14,22},{16,24},... | collective-permute-start | bytes 2359304 | tf_op jit(solution)/shard_map/ppermute | solution.py:16
  119.0 3.1 collective-permute-start.1
  132.4 6.3 copy.17
  141.7 11.9 %collective-permute-done.2 = bf16[384,1024]{1,0:T(8,128)(2,1)S(1)} collective-permute-done((bf16[384,1024]{1,0:T(8,128)(2,1)S(1)}, bf16[384,1024]{1,0:T(8,128)(2,1)S(1)}, u32[]{:S(2)}, u32[]{:S(2)}) %collective-permute-start.2) | collective-permute-done | bytes 786464 | tf_op jit(solution)/shard_map/ppermute | solution.py:16
  157.6 6.4 copy.16
  164.1 26.9 %fusion.22 = (f32[16,384]{1,0:T(8,128)S(1)}, f32[16,384,1920]{1,2,0:T(8,128)}) fusion(f32[16,1920]{1,0:T(8,128)S(1)} %bitcast.33, f32[16,384]{1,0:T(8,128)S(1)} %bitcast.32, pred[384,1920]{0,1:T(8,128)(4,1)S(1)} %copy-done.3, bf16[1920,16,64]{0,2,1:T(8,128)(2,1)} %bitcast.29, bf16[384,16,64]{0,2,1:T(8,128)(2,1)S(1)} %bitcast.31), kind=kOutput, calls=%fused_computation.53 | convolution fusion | flops 1580730240 | bytes 52813824 | tf_op jit(solution)/shard_map/sub | solution.py:76
  190.9 17.4 %fusion.14 = bf16[16,64,384]{2,1,0:T(8,128)(2,1)S(1)} fusion(bf16[1920,16,64]{0,2,1:T(8,128)(2,1)} %bitcast.30, f32[16,384,1920]{1,2,0:T(8,128)} %get-tuple-element.8, f32[16,384]{1,0:T(8,128)S(1)} %get-tuple-element.7), kind=kOutput, calls=%fused_computation.24 | convolution fusion | flops 1533935616 | bytes 51929088 | tf_op jit(solution)/shard_map/hqk,khd->qhd/dot_general | solution.py:78
  208.3 3.0 convolution_convert_fusion
  213.4 43.0 %all-reduce.2.cloned.1.call-done = bf16[384,2048]{1,0:T(8,128)(2,1)} async-done(((bf16[384,2048]{1,0:T(8,128)(2,1)}), bf16[384,2048]{1,0:T(8,128)(2,1)}) %all-reduce.2.cloned.1.call-update) | async-done | bytes 1572880 | tf_op jit(solution)/shard_map/psum | solution.py:83
  258.5 111.8 %all-gather.4.cloned.1.call-done = bf16[2048,2560]{1,0:T(8,128)(2,1)} async-done(((bf16[128,2560]{1,0:T(8,128)(2,1)}), bf16[2048,2560]{1,0:T(8,128)(2,1)}) %all-gather.4.cloned.1.call-update) | async-done | bytes 10485776 | tf_op jit(solution)/shard_map/all_gather | solution.py:88
  370.3 8.9 %fusion.17 = f32[384,2560]{1,0:T(8,128)} fusion(bf16[2048,2560]{1,0:T(8,128)(2,1)} %all-gather.4.cloned.1.call-done, bf16[384,2048]{1,0:T(8,128)(2,1)S(1)} %get-tuple-element.6, f32[2048]{0:T(1024)S(1)} %copy-done.6, f32[384]{0:T(512)S(1)} %add_rsqrt_fusion), kind=kOutput, calls=%fused_computation.25 | convolution fusion | flops 4029677568 | bytes 16000512 | tf_op jit(solution)/shard_map/dot_general | solution.py:91
  379.2 123.1 %all-gather.6.cloned.1.call-done = bf16[2048,2560]{1,0:T(8,128)(2,1)} async-done(((bf16[128,2560]{1,0:T(8,128)(2,1)}), bf16[2048,2560]{1,0:T(8,128)(2,1)}) %all-gather.6.cloned.1.call-update) | async-done | bytes 10485776 | tf_op jit(solution)/shard_map/all_gather | solution.py:89
  502.3 169.3 %all-gather.8.cloned.1.call-done = bf16[2560,2048]{1,0:T(8,128)(2,1)} async-done(((bf16[2560,128]{1,0:T(8,128)(2,1)}), bf16[2560,2048]{1,0:T(8,128)(2,1)}) %all-gather.8.cloned.1.call-update) | async-done | bytes 10485776 | tf_op jit(solution)/shard_map/all_gather | solution.py:96
  671.5 17.7 %convolution_convert_fusion.1 = bf16[384,2048]{1,0:T(8,128)(2,1)} fusion(bf16[2560,2048]{1,0:T(8,128)(2,1)} %all-gather.8.cloned.1.call-done, bf16[2048,2560]{1,0:T(8,128)(2,1)} %all-gather.6.cloned.1.call-done, f32[384,2560]{1,0:T(8,128)} %fusion.17, bf16[384,2048]{1,0:T(8,128)(2,1)S(1)} %get-tuple-element.6, f32[2048]{0:T(1024)S(1)} %copy-done.6, ...), kind=kOutput, calls=%fused_computation.22 | convolution fusion | flops 8062894080 | bytes 28059136 | tf_op jit(solution)/shard_map/dot_general | solution.py:94
  689.3 7.4 %reduce-scatter.2.cloned.1.call-done = bf16[192,2048]{1,0:T(8,128)(2,1)} async-done(((bf16[384,2048]{1,0:T(8,128)(2,1)}), bf16[192,2048]{1,0:T(8,128)(2,1)}) %reduce-scatter.2.cloned.1.call-update) | async-done | bytes 786448 | tf_op jit(solution)/shard_map/reduce_scatter | solution.py:99
  (73 shorter events, 39.1 us)
Async XLA Ops:
  7.4 115.6 %copy-start.2 = (bf16[384,1024]{1,0:T(8,128)(2,1)S(1)}, bf16[384,1024]{1,0:T(8,128)(2,1)}, u32[]{:S(2)}) copy-start(bf16[384,1024]{1,0:T(8,128)(2,1)} %param.14) | copy-start | bytes 2359300
  7.4 249.0 %all-reduce.2.cloned.1.call-start = ((), (), s32[]{:S(2)}) async-start(), calls=%async_computation.1 | async-start | bytes 3145728 | tf_op jit(solution)/shard_map/psum | solution.py:83
  7.4 20.5 %collective-permute-start.4 = (s32[384]{0:T(512)}, s32[384]{0:T(512)S(1)}, u32[]{:S(2)}, u32[]{:S(2)}) collective-permute-start(s32[384]{0:T(512)} %param.16), channel_id=1, source_target_pairs={{0,8},{2,10},{4,12},{6,14},{8,16},{10,18},{12,20},{14,22},{16,24},... | collective-permute-start | bytes 4616 | tf_op jit(solution)/shard_map/ppermute | solution.py:16
  12.5 19.4 %collective-permute-start.5 = (s32[384]{0:T(512)}, s32[384]{0:T(512)S(1)}, u32[]{:S(2)}, u32[]{:S(2)}) collective-permute-start(s32[384]{0:T(512)} %param.16), channel_id=1, source_target_pairs={{0,6},{2,8},{4,10},{6,12},{8,14},{10,16},{12,18},{14,20},{16,22},{... | collective-permute-start | bytes 4616 | tf_op jit(solution)/shard_map/ppermute | solution.py:16
  16.8 18.4 %collective-permute-start.6 = (s32[384]{0:T(512)}, s32[384]{0:T(512)S(1)}, u32[]{:S(2)}, u32[]{:S(2)}) collective-permute-start(s32[384]{0:T(512)} %param.16), channel_id=1, source_target_pairs={{0,4},{2,6},{4,8},{6,10},{8,12},{10,14},{12,16},{14,18},{16,20},{1... | collective-permute-start | bytes 4616 | tf_op jit(solution)/shard_map/ppermute | solution.py:16
  20.3 16.4 %collective-permute-start.7 = (s32[384]{0:T(512)}, s32[384]{0:T(512)S(1)}, u32[]{:S(2)}, u32[]{:S(2)}) collective-permute-start(s32[384]{0:T(512)} %param.16), channel_id=1, source_target_pairs={{0,2},{2,4},{4,6},{6,8},{8,10},{10,12},{12,14},{14,16},{16,18},{18... | collective-permute-start | bytes 4616 | tf_op jit(solution)/shard_map/ppermute | solution.py:16
  22.8 96.2 %collective-permute-start.8 = (bf16[384,1024]{1,0:T(8,128)(2,1)}, bf16[384,1024]{1,0:T(8,128)(2,1)S(1)}, u32[]{:S(2)}, u32[]{:S(2)}) collective-permute-start(bf16[384,1024]{1,0:T(8,128)(2,1)} %param.13), channel_id=1, source_target_pairs={{0,8},{2,10},{4,12},{6,14},{8,16},{10,18},{12,20},{14,22},{16,24},... | collective-permute-start | bytes 2359304 | tf_op jit(solution)/shard_map/ppermute | solution.py:16
  27.9 103.6 %copy-start.1 = (bf16[384,1024]{1,0:T(8,128)(2,1)S(1)}, bf16[384,1024]{1,0:T(8,128)(2,1)}, u32[]{:S(2)}) copy-start(bf16[384,1024]{1,0:T(8,128)(2,1)} %param.13) | copy-start | bytes 2359300
  27.9 95.1 %collective-permute-start.9 = (bf16[384,1024]{1,0:T(8,128)(2,1)}, bf16[384,1024]{1,0:T(8,128)(2,1)S(1)}, u32[]{:S(2)}, u32[]{:S(2)}) collective-permute-start(bf16[384,1024]{1,0:T(8,128)(2,1)} %param.13), channel_id=1, source_target_pairs={{0,6},{2,8},{4,10},{6,12},{8,14},{10,16},{12,18},{14,20},{16,22},{... | collective-permute-start | bytes 2359304 | tf_op jit(solution)/shard_map/ppermute | solution.py:16
  31.8 94.9 %collective-permute-start.10 = (bf16[384,1024]{1,0:T(8,128)(2,1)}, bf16[384,1024]{1,0:T(8,128)(2,1)S(1)}, u32[]{:S(2)}, u32[]{:S(2)}) collective-permute-start(bf16[384,1024]{1,0:T(8,128)(2,1)} %param.13), channel_id=1, source_target_pairs={{0,4},{2,6},{4,8},{6,10},{8,12},{10,14},{12,16},{14,18},{16,20},{1... | collective-permute-start | bytes 2359304 | tf_op jit(solution)/shard_map/ppermute | solution.py:16
  35.3 95.2 %collective-permute-start.11 = (bf16[384,1024]{1,0:T(8,128)(2,1)}, bf16[384,1024]{1,0:T(8,128)(2,1)S(1)}, u32[]{:S(2)}, u32[]{:S(2)}) collective-permute-start(bf16[384,1024]{1,0:T(8,128)(2,1)} %param.13), channel_id=1, source_target_pairs={{0,2},{2,4},{4,6},{6,8},{8,10},{10,12},{12,14},{14,16},{16,18},{18... | collective-permute-start | bytes 2359304 | tf_op jit(solution)/shard_map/ppermute | solution.py:16
  36.6 6.0 collective-permute-start.12
  42.7 56.3 %collective-permute-start.13 = (f32[384,16]{0,1:T(8,128)}, f32[384,16]{0,1:T(8,128)S(1)}, u32[]{:S(2)}, u32[]{:S(2)}) collective-permute-start(f32[384,16]{0,1:T(8,128)} %param.15), channel_id=1, source_target_pairs={{0,6},{2,8},{4,10},{6,12},{8,14},{10,16},{12,18},{14,20},{16,22},{... | collective-permute-start | bytes 73736 | tf_op jit(solution)/shard_map/ppermute | solution.py:16
  99.0 3.0 collective-permute-start.14
  102.0 8.0 %collective-permute-start.15 = (f32[384,16]{0,1:T(8,128)}, f32[384,16]{0,1:T(8,128)S(1)}, u32[]{:S(2)}, u32[]{:S(2)}) collective-permute-start(f32[384,16]{0,1:T(8,128)} %param.15), channel_id=1, source_target_pairs={{0,2},{2,4},{4,6},{6,8},{8,10},{10,12},{12,14},{14,16},{16,18},{18... | collective-permute-start | bytes 73736 | tf_op jit(solution)/shard_map/ppermute | solution.py:16
  110.0 28.7 %collective-permute-start = (bf16[384,1024]{1,0:T(8,128)(2,1)}, bf16[384,1024]{1,0:T(8,128)(2,1)S(1)}, u32[]{:S(2)}, u32[]{:S(2)}) collective-permute-start(bf16[384,1024]{1,0:T(8,128)(2,1)} %param.14), channel_id=1, source_target_pairs={{0,8},{2,10},{4,12},{6,14},{8,16},{10,18},{12,20},{14,22},{16,24},... | collective-permute-start | bytes 2359304 | tf_op jit(solution)/shard_map/ppermute | solution.py:16
  119.0 20.6 %collective-permute-start.1 = (bf16[384,1024]{1,0:T(8,128)(2,1)}, bf16[384,1024]{1,0:T(8,128)(2,1)}, u32[]{:S(2)}, u32[]{:S(2)}) collective-permute-start(bf16[384,1024]{1,0:T(8,128)(2,1)} %param.14), channel_id=1, source_target_pairs={{0,6},{2,8},{4,10},{6,12},{8,14},{10,16},{12,18},{14,20},{16,22},{... | collective-permute-start | bytes 2359304 | tf_op jit(solution)/shard_map/ppermute | solution.py:16
  123.0 30.7 %collective-permute-start.2 = (bf16[384,1024]{1,0:T(8,128)(2,1)S(1)}, bf16[384,1024]{1,0:T(8,128)(2,1)S(1)}, u32[]{:S(2)}, u32[]{:S(2)}) collective-permute-start(bf16[384,1024]{1,0:T(8,128)(2,1)S(1)} %copy-done.2), channel_id=1, source_target_pairs={{0,4},{2,6},{4,8},{6,10},{8,12},{10,14},{12,16},{14,18},{16,20},{1... | collective-permute-start | bytes 2359304 | tf_op jit(solution)/shard_map/ppermute | solution.py:16
  126.8 27.8 %collective-permute-start.3 = (bf16[384,1024]{1,0:T(8,128)(2,1)S(1)}, bf16[384,1024]{1,0:T(8,128)(2,1)}, u32[]{:S(2)}, u32[]{:S(2)}) collective-permute-start(bf16[384,1024]{1,0:T(8,128)(2,1)S(1)} %copy-done.2), channel_id=1, source_target_pairs={{0,2},{2,4},{4,6},{6,8},{8,10},{10,12},{12,14},{14,16},{16,18},{18... | collective-permute-start | bytes 2359304 | tf_op jit(solution)/shard_map/ppermute | solution.py:16
  211.4 158.9 %copy-start.6 = (f32[2048]{0:T(1024)S(1)}, f32[2048]{0:T(1024)}, u32[]{:S(2)}) copy-start(f32[2048]{0:T(1024)} %param.18) | copy-start | bytes 24580
  211.4 158.9 %all-gather.4.cloned.1.call-start = ((), (), s32[]{:S(2)}) async-start(), calls=%async_computation.2 | async-start | bytes 11141120 | tf_op jit(solution)/shard_map/all_gather | solution.py:88
  212.0 290.3 %all-gather.6.cloned.1.call-start = ((), (), s32[]{:S(2)}) async-start(), calls=%async_computation.3 | async-start | bytes 11141120 | tf_op jit(solution)/shard_map/all_gather | solution.py:89
  212.6 459.0 %all-gather.8.cloned.1.call-start = ((), (), s32[]{:S(2)}) async-start(), calls=%async_computation.4 | async-start | bytes 11141120 | tf_op jit(solution)/shard_map/all_gather | solution.py:96
  213.1 483.5 %reduce-scatter.2.cloned.1.call-start = ((), (), s32[]{:S(2)}) async-start(), calls=%async_computation.5 | async-start | bytes 2359296 | tf_op jit(solution)/shard_map/reduce_scatter | solution.py:99
  (4 other events, 75.2 us)
Sparse Core Ops, SparseCore 0:
  211.5 44.7 all-reduce.1
  689.4 7.2 reduce-scatter.1
Sparse Core Ops, SparseCore 1:
  214.6 155.6 all-gather.3
  372.8 129.4 all-gather.5
  504.9 166.6 all-gather.7
where the time goes:
time: 708 us; the launch traced here: 707 us
  waiting for transfers between devices  473 us (67%)
  starting transfers between devices  109 us (15%)
  matrix products  73.9 us (10%)
  local copies, waits for them, and re-layouts  27.4 us (4%)
  between operations  15.3 us (2%)
  other arithmetic  7.69 us (1%)
    all_gather x1, waiting for transfers between devices, local(): lax.all_gather(down_weight, 'sp', axis=1, tiled=True)  169 us
    all_gather x1, waiting for transfers between devices, local(): lax.all_gather(up_weight, 'sp', axis=0, tiled=True)  123 us
    all_gather x1, waiting for transfers between devices, local(): lax.all_gather(gate_weight, 'sp', axis=0, tiled=True)  112 us
    ppermute x16, starting transfers between devices, from_behind(): lax.ppermute(value, axis, [(source, source + steps) for source in range(f...  108 us
    psum x1, waiting for transfers between devices, local(): lax.psum(partial_value.astype(jnp.bfloat16), 'tp').astype(jnp.float32)  43 us
    sub x1, matrix products, local(): exp_scores = jnp.exp(scores - row_max)  26.9 us
    dot_general x1, matrix products, local(): jnp.dot(hidden, lax.all_gather(down_weight, 'sp', axis=1, tiled=True), pr...  17.7 us
    dot_general x1, matrix products, local(): jnp.einsum('hqk,khd->qhd', weights, value_heads, preferred_element_type=j...  17.4 us
  transfers between devices with their start and end apart: 21, of which 10 were waited for; matrix products, arithmetic and copies ran while one was open for 5% of the time, Pallas kernels for 0%

commit v1 on v0

v1 whole, which is shorter than its diff:
```python
import functools

import jax
import jax.numpy as jnp
from jax import lax
from jax.experimental import pallas as pl
from jax.experimental.pallas import tpu as pltpu
from jax.sharding import PartitionSpec as P

REACH = 4

EPSILON = 1e-06
NEGATIVE = -1e30
LANES = 128


WHOLE = pl.BlockSpec(memory_space=pltpu.VMEM)


def attend_kernel(where_ref, *refs, group, heads, scale):
    qs, kvs, olds, auxes = (refs[i * group : (i + 1) * group] for i in range(4))
    outs = refs[4 * group : 5 * group]
    q_ref, kv_ref, aux_ref, acc_ref = refs[5 * group :]
    rows, width = q_ref.shape
    head_size = width // heads
    member = where_ref[0]
    step = pl.program_id(0)

    @pl.when(step == 0)
    def _():
        for mask in range(group):
            other = member ^ mask
            kv_ref[other] = olds[mask][...]
            kv_ref[group + other] = kvs[mask][...]
            aux = auxes[mask]
            aux_ref[other] = aux[0]
            aux_ref[group + other] = aux[1]

    for mask in range(group):

        @pl.when(step == member ^ mask)
        def _(mask=mask):
            q_ref[...] = qs[mask][...] * jnp.asarray(scale, q_ref.dtype)

    lane = lax.broadcasted_iota(jnp.int32, (1, width), 1) // head_size
    q = q_ref[...]
    q_parts = [jnp.where(lane == h, q, jnp.zeros_like(q)) for h in range(heads)]
    last = aux_ref.shape[1] - 1
    diagonal = group + step
    own_docs = aux_ref[diagonal, last : last + 1, :]
    first_doc = jnp.min(own_docs)
    qdoc = jnp.transpose(jnp.broadcast_to(own_docs, (128, rows)))[:, :1]
    low = step
    for back in range(group):
        before = jnp.max(aux_ref[step + back, last : last + 1, :]) < first_doc
        low = low + before.astype(jnp.int32)
    acc_ref[...] = jnp.zeros_like(acc_ref)

    def chunk(index, carry, causal):
        k = kv_ref[index, :, :width]
        v = kv_ref[index, :, width:]
        seen = aux_ref[index, last : last + 1, :] == qdoc
        if causal:
            row = lax.broadcasted_iota(jnp.int32, (rows, rows), 0)
            col = lax.broadcasted_iota(jnp.int32, (rows, rows), 1)
            seen = seen & (col <= row)
        new = []
        decay = jnp.zeros((rows, width), jnp.float32)
        added = jnp.zeros((rows, width), jnp.float32)
        for h in range(heads):
            top, total = carry[h]
            gate = aux_ref[index, pl.ds(member * heads + h, 1), :]
            scores = lax.dot_general(
                q_parts[h], k, (((1,), (1,)), ((), ())), preferred_element_type=jnp.float32
            )
            scores = jnp.where(seen, scores - gate, NEGATIVE)
            new_top = jnp.maximum(top, jnp.max(scores, axis=-1, keepdims=True))
            weights = jnp.exp(scores - new_top)
            shrink = jnp.exp(top - new_top)
            total = total * shrink + jnp.sum(weights, axis=-1, keepdims=True)
            v_part = jnp.where(lane == h, v, jnp.zeros_like(v))
            added = added + jnp.dot(
                weights.astype(v.dtype), v_part, preferred_element_type=jnp.float32
            )
            decay = jnp.where(lane == h, shrink, decay)
            new.append((new_top, total))
        acc_ref[...] = acc_ref[...] * decay + added
        return tuple(new)

    first = tuple(
        (jnp.full((rows, 1), NEGATIVE, jnp.float32), jnp.zeros((rows, 1), jnp.float32))
        for _ in range(heads)
    )
    carry = lax.fori_loop(low, diagonal, functools.partial(chunk, causal=False), first)
    carry = chunk(diagonal, carry, True)
    divisor = jnp.ones((rows, width), jnp.float32)
    for h in range(heads):
        divisor = jnp.where(lane == h, carry[h][1], divisor)
    value = (acc_ref[...] / divisor).astype(jnp.bfloat16)
    for mask in range(group):

        @pl.when(step == member ^ mask)
        def _(mask=mask):
            outs[mask][...] = value


def attend(member, qs, kvs, olds, auxes, heads, scale):
    group = len(qs)
    rows, width = qs[0].shape
    aux_shape = (2 * group,) + auxes[0].shape[1:]
    span = group * rows
    return pl.pallas_call(
        functools.partial(attend_kernel, group=group, heads=heads, scale=scale),
        grid=(group,),
        in_specs=[pl.BlockSpec(memory_space=pltpu.SMEM)] + [WHOLE] * (4 * group),
        out_specs=[WHOLE] * group,
        scratch_shapes=[
            pltpu.VMEM((rows, width), jnp.bfloat16),
            pltpu.VMEM((2 * group, rows, 2 * width), jnp.bfloat16),
            pltpu.VMEM(aux_shape, jnp.float32),
            pltpu.VMEM((rows, width), jnp.float32),
        ],
        out_shape=[jax.ShapeDtypeStruct((rows, width), jnp.bfloat16)] * group,
        cost_estimate=pl.CostEstimate(
            flops=4 * span * span * width * heads,
            bytes_accessed=8 * span * width * 2,
            transcendentals=span * span * heads,
        ),
        name="attend",
    )(member[None], *qs, *kvs, *olds, *auxes)


def project_kernel(where_ref, *refs, group, parts):
    member, place = where_ref[0], where_ref[1]
    pieces, weight_ref, outs = refs[:group], refs[group], refs[group + 1 :]
    rows, width = pieces[0].shape
    own = rows // parts
    for part in range(parts):
        start = pl.multiple_of(lax.rem(place + part, parts) * own, own)
        total = None
        for mask in range(group):
            at = pl.multiple_of((member ^ mask) * width, width)
            term = jnp.dot(
                pieces[mask][pl.ds(start, own), :],
                weight_ref[pl.ds(at, width), :],
                preferred_element_type=jnp.float32,
            )
            total = term if total is None else total + term
        outs[part][...] = total.astype(jnp.bfloat16)


def project(member, place, pieces, weight, parts):
    group = len(pieces)
    rows, width = pieces[0].shape
    features = weight.shape[1]
    block = features // 4
    own = rows // parts
    return pl.pallas_call(
        functools.partial(project_kernel, group=group, parts=parts),
        grid=(4,),
        in_specs=[pl.BlockSpec(memory_space=pltpu.SMEM)]
        + [WHOLE] * group
        + [pl.BlockSpec((weight.shape[0], block), lambda i: (0, i))],
        out_specs=[pl.BlockSpec((own, block), lambda i: (0, i))] * parts,
        out_shape=[jax.ShapeDtypeStruct((own, features), jnp.bfloat16)] * parts,
        cost_estimate=pl.CostEstimate(
            flops=2 * rows * width * group * features,
            bytes_accessed=2 * weight.size,
            transcendentals=0,
        ),
        name="project",
    )(jnp.stack([member, place]), *pieces, weight)


def middle_kernel(where_ref, residual_ref, *refs, parts, levels, group):
    device, place = where_ref[0], where_ref[1]
    partials, gain_ref = refs[:parts], refs[parts]
    middle_ref, mine_ref, theirs_ref, normed_ref = refs[parts + 1 :]
    own = middle_ref.shape[0]
    total = partials[0][...].astype(jnp.float32)
    for part in partials[1:]:
        total = total + part[...].astype(jnp.float32)
    start = pl.multiple_of(place * own, own)
    middle = (residual_ref[pl.ds(start, own), :].astype(jnp.float32) + total).astype(jnp.bfloat16)
    middle_ref[...] = middle
    widened = middle.astype(jnp.float32)
    factor = lax.rsqrt(jnp.mean(widened * widened, axis=-1, keepdims=True) + EPSILON)
    normed_ref[...] = (widened * factor * gain_ref[...]).astype(jnp.bfloat16)
    depth = middle_ref.shape[1] // (levels * group)
    if depth % LANES:
        mine_ref[...] = normed_ref[...]
        theirs_ref[...] = normed_ref[...]
        return
    for mask in range(group):
        for level in range(levels):
            source = device ^ (level * group + mask)
            block = normed_ref[:, pl.ds(pl.multiple_of(source * depth, depth), depth)]
            at = (mask * levels + level) * depth
            mine_ref[:, at : at + depth] = block
            at = (mask * levels + (level ^ 1)) * depth
            theirs_ref[:, at : at + depth] = block


def make_middle(device, place, residual, partials, gain, levels, group):
    own, features = partials[0].shape
    shape = jax.ShapeDtypeStruct((own, features), jnp.bfloat16)
    middle, mine, theirs = pl.pallas_call(
        functools.partial(middle_kernel, parts=len(partials), levels=levels, group=group),
        in_specs=[pl.BlockSpec(memory_space=pltpu.SMEM)] + [WHOLE] * (len(partials) + 2),
        out_specs=[WHOLE] * 3,
        out_shape=[shape] * 3,
        scratch_shapes=[pltpu.VMEM((own, features), jnp.bfloat16)],
        cost_estimate=pl.CostEstimate(
            flops=2000 * own * features, bytes_accessed=10 * own * features, transcendentals=own
        ),
        name="middle",
    )(jnp.stack([device, place]), residual, *partials, gain[None])
    depth = features // (levels * group)
    if depth % LANES:
        order = jnp.arange(levels * group, dtype=jnp.int32)
        mask, kept = order // levels, order % levels
        blocks = mine.reshape(own, levels * group, depth)
        mine = jnp.take(blocks, device ^ (kept * group + mask), axis=1).reshape(own, features)
        theirs = jnp.take(blocks, device ^ ((kept ^ 1) * group + mask), axis=1)
        theirs = theirs.reshape(own, features)
    return middle, mine, theirs


def mix_kernel(*refs, blocks, offsets):
    count = len(offsets)
    xs, gates, ups = refs[:blocks], refs[blocks : blocks + count], refs[blocks + count : blocks + 2 * count]
    out_ref, x_ref = refs[blocks + 2 * count :]
    own = xs[0].shape[0]

    @pl.when(pl.program_id(0) == 0)
    def _():
        for index in range(blocks):
            x_ref[index * own : (index + 1) * own, :] = xs[index][...]

    def product(parts):
        total = None
        for offset, part in zip(offsets, parts):
            term = jnp.dot(
                x_ref[:, offset : offset + part.shape[0]],
                part[...],
                preferred_element_type=jnp.float32,
            )
            total = term if total is None else total + term
        return total

    gate, up = product(gates), product(ups)
    out_ref[...] = (gate / (1.0 + jnp.exp(-gate)) * up).astype(jnp.bfloat16)


def mix(xs, gates, ups):
    own, features = xs[0].shape
    rows = own * len(xs)
    hidden = gates[0].shape[1]
    block = next(size for size in (256, 128, hidden) if hidden % size == 0)
    offsets, at = [], 0
    for part in gates:
        offsets.append(at)
        at += part.shape[0]
    weights = [pl.BlockSpec((part.shape[0], block), lambda i: (0, i)) for part in gates]
    return pl.pallas_call(
        functools.partial(mix_kernel, blocks=len(xs), offsets=tuple(offsets)),
        grid=(hidden // block,),
        in_specs=[WHOLE] * len(xs) + weights + weights,
        out_specs=pl.BlockSpec((rows, block), lambda i: (0, i)),
        out_shape=jax.ShapeDtypeStruct((rows, hidden), jnp.bfloat16),
        scratch_shapes=[pltpu.VMEM((rows, features), jnp.bfloat16)],
        cost_estimate=pl.CostEstimate(
            flops=4 * rows * features * hidden,
            bytes_accessed=4 * features * hidden + 2 * rows * (features + hidden),
            transcendentals=rows * hidden,
        ),
        name="mix",
    )(*xs, *gates, *ups)


def final_kernel(where_ref, middle_ref, *refs, levels, group, shapes):
    device = where_ref[0]
    kept, got, out_ref = refs[: len(shapes)], refs[len(shapes) : 2 * len(shapes)], refs[-1]
    depth = middle_ref.shape[1] // (levels * group)
    for index, (mask, first) in enumerate(shapes):
        for column in range(kept[index].shape[1] // depth):
            level = first + column
            at = pl.ds(pl.multiple_of((device ^ (level * group + mask)) * depth, depth), depth)
            mine = slice(column * depth, (column + 1) * depth)
            theirs = slice((column ^ 1) * depth, ((column ^ 1) + 1) * depth)
            total = kept[index][:, mine] + got[index][:, theirs].astype(jnp.float32)
            out_ref[:, at] = (middle_ref[:, at].astype(jnp.float32) + total).astype(out_ref.dtype)


def finish(device, middle, kept, got, shapes, levels, group):
    own, features = middle.shape
    depth = features // (levels * group)
    if depth % LANES:
        place = device ^ jnp.arange(levels * group, dtype=jnp.int32)
        mask, column = place % group, place // group
        kept = jnp.concatenate(kept, axis=1).reshape(own, -1, depth)
        got = jnp.concatenate(got, axis=1).reshape(own, -1, depth).astype(jnp.float32)
        total = jnp.take(kept, mask * levels + column, axis=1)
        total = total + jnp.take(got, mask * levels + (column ^ 1), axis=1)
        return (middle.astype(jnp.float32) + total.reshape(own, features)).astype(middle.dtype)
    return pl.pallas_call(
        functools.partial(final_kernel, levels=levels, group=group, shapes=tuple(shapes)),
        in_specs=[pl.BlockSpec(memory_space=pltpu.SMEM)] + [WHOLE] * (1 + 2 * len(shapes)),
        out_specs=WHOLE,
        out_shape=jax.ShapeDtypeStruct(middle.shape, middle.dtype),
        cost_estimate=pl.CostEstimate(
            flops=2000 * middle.size, bytes_accessed=10 * middle.size, transcendentals=0
        ),
        name="finish",
    )(device[None], middle, *kept, *got)


def local(
    residual,
    queries,
    keys,
    values,
    gate_cache,
    doc_ids,
    out_weight,
    mix_gain,
    gate_weight,
    up_weight,
    down_weight,
):
    n_sp, n_tp = lax.axis_size("sp"), lax.axis_size("tp")
    group = REACH
    levels = n_sp // group
    sp_index, tp_index = lax.axis_index("sp"), lax.axis_index("tp")
    level, member = sp_index // group, sp_index % group
    rows, width = queries.shape
    heads_here = gate_cache.shape[1]
    head_size = width // heads_here
    heads = heads_here // group
    share = width // group
    own = rows // n_tp

    def swap(value, mask):
        return lax.ppermute(value, "sp", [(s, s ^ mask) for s in range(n_sp)])

    def next_level(value):
        return lax.ppermute(value, "sp", [(s, s + group) for s in range(n_sp - group)])

    def turn(value, steps):
        return lax.ppermute(value, "tp", [(t, (t + steps) % n_tp) for t in range(n_tp)])

    def piece(value, index, size, axis):
        return lax.dynamic_slice_in_dim(value, index * size, size, axis)

    def cut_kv(other):
        return jnp.concatenate(
            [piece(keys, other, share, 1), piece(values, other, share, 1)], axis=1
        )

    others = range(1, group)
    kvs = [cut_kv(member)] + [swap(cut_kv(member ^ m), m) for m in others]
    olds = [next_level(kvs[m]) for m in range(group)]
    qs = [piece(queries, member, share, 1)]
    qs += [swap(piece(queries, member ^ m, share, 1), m) for m in others]
    marks = jnp.concatenate([gate_cache.T, doc_ids.astype(jnp.float32)[None] + 1.0], axis=0)
    marks = jnp.stack([next_level(marks), marks])
    auxes = [marks] + [swap(marks, m) for m in others]

    half = gate_weight.shape[1] // 2
    parity = level % 2

    def from_levels(weight, axis):
        kept = piece(weight, parity, half, axis)
        given = piece(weight, 1 - parity, half, axis)
        parts = [kept]
        for distance in range(1, levels):
            parts.append(swap(given if distance % 2 else kept, distance * group))
        return jnp.concatenate(parts, axis=1 - axis)

    def from_members(weight, axis):
        middle = weight.shape[axis] // 2
        along_x, along_y = swap(weight, 1), swap(weight, 2)
        near = swap(lax.slice_in_dim(along_y, 0, middle, axis=axis), 1)
        far = swap(lax.slice_in_dim(along_x, middle, 2 * middle, axis=axis), 2)
        return [weight, along_x, along_y, near, far]

    gates = from_members(from_levels(gate_weight, 1), 0)
    ups = from_members(from_levels(up_weight, 1), 0)
    downs = from_members(from_levels(down_weight, 0), 1)

    attended = attend(member, qs, kvs, olds, auxes, heads, head_size ** (-0.5))

    pieces = [attended[0]] + [swap(attended[m], m) for m in others]
    partials = project(member, tp_index, pieces, out_weight, n_tp)
    partials = [partials[0]] + [turn(partials[steps], steps) for steps in range(1, n_tp)]
    middle, mine, theirs = make_middle(
        sp_index, tp_index, residual, partials, mix_gain, levels, group
    )

    theirs = swap(theirs, group)
    xs = [mine] + [turn(mine, steps) for steps in range(1, n_tp)]
    xs += [theirs] + [turn(theirs, steps) for steps in range(1, n_tp)]
    hidden = mix(xs, gates, ups)

    kept, got, shapes = [], [], []
    for index, (mask, first) in enumerate(((0, 0), (1, 0), (2, 0), (3, 0), (3, levels // 2))):
        lowered = jnp.dot(hidden, downs[index], preferred_element_type=jnp.float32)
        lowered = lowered.reshape(2, n_tp, own, -1)
        total = lowered[:, 0]
        for steps in range(1, n_tp):
            sent = lowered[:, steps].astype(jnp.bfloat16)
            total = total + turn(sent, -steps).astype(jnp.float32)
        kept.append(total[0])
        got.append(swap(total[1].astype(jnp.bfloat16), group))
        shapes.append((mask, first))
    return finish(sp_index, middle, kept, got, shapes, levels, group)


def solution(mesh):
    return jax.shard_map(
        local,
        mesh=mesh,
        in_specs=(
            P("sp", None),
            P("sp", "tp"),
            P("sp", "tp"),
            P("sp", "tp"),
            P("sp", "tp"),
            P("sp"),
            P("tp", None),
            P(),
            P("sp", "tp"),
            P("sp", "tp"),
            P("tp", "sp"),
        ),
        out_specs=P(("sp", "tp"), None),
        check_vma=False,
    )
```

time: 708 us -> 319 us (0.45)
  waiting for transfers between devices: 473 us -> 136 us
  matrix products: 73.9 us -> 11.4 us
  Pallas kernels: 0 us -> 49.2 us
  between operations: 15.3 us -> 0.67 us
  starting transfers between devices: 109 us -> 95.2 us
    all_gather x3 -> x0, waiting for transfers between devices: 404 us -> none  [the longest x1 169 us: local(): lax.all_gather(down_weight, 'sp', axis=1, tiled=True)]
    ppermute x16 -> x52, waiting for transfers between devices: 17.4 us -> 136 us  [the longest x39 124 us: swap(): return lax.ppermute(value, 'sp', [(s, s ^ mask) for s in range(n_sp)])]
    pallas_call x0 -> x5, Pallas kernels: none -> 49.2 us  [the longest x1 23.7 us: attend(): pl.pallas_call(functools.partial(attend_kernel, group=group, heads=heads,...]
    psum x1 -> x0, waiting for transfers between devices: 43 us -> none  [local(): lax.psum(partial_value.astype(jnp.bfloat16), 'tp').astype(jnp.float32)]
    dot_general x4 -> x5, matrix products: 47.1 us -> 11.4 us  [local(): lowered = jnp.dot(hidden, downs[index], preferred_element_type=jnp.float32)]
    sub x1 -> x0, matrix products: 26.9 us -> none  [local(): exp_scores = jnp.exp(scores - row_max)]
    concatenate x6 -> x0, local copies, waits for them, and re-layouts: 16 us -> none  [the longest x2 7.35 us: local(): all_values = jnp.concatenate(value_parts[::-1], axis=0)]
    ppermute x16 -> x52, starting transfers between devices: 108 us -> 95.2 us  [the longest x39 77.5 us: swap(): return lax.ppermute(value, 'sp', [(s, s ^ mask) for s in range(n_sp)])]
  transfers between devices with their start and end apart: 21 -> 52, of which waited for: 10 -> 22; matrix products, arithmetic and copies ran while one was open for 5% -> 10% of each run, Pallas kernels for 0% -> 14%
where the time goes in v1:
time: 319 us
  waiting for transfers between devices  136 us (43%)
  starting transfers between devices  95.2 us (30%)
  Pallas kernels  49.2 us (15%)
  local copies, waits for them, and re-layouts  20.4 us (6%)
  matrix products  11.4 us (4%)
  other arithmetic  6.33 us (2%)
    ppermute x39, waiting for transfers between devices, swap(): return lax.ppermute(value, 'sp', [(s, s ^ mask) for s in range(n_sp)])  124 us
    ppermute x39, starting transfers between devices, swap(): return lax.ppermute(value, 'sp', [(s, s ^ mask) for s in range(n_sp)])  77.5 us
    pallas_call x1, Pallas kernels, attend(): pl.pallas_call(functools.partial(attend_kernel, group=group, heads=heads,...  23.7 us
    ppermute x5, starting transfers between devices, next_level(): lax.ppermute(value, 'sp', [(s, s + group) for s in range(n_sp - group)])  15.9 us
    pallas_call x1, Pallas kernels, mix(): pl.pallas_call(functools.partial(mix_kernel, blocks=len(xs), offsets=tupl...  13.2 us
    ppermute x5, waiting for transfers between devices, next_level(): lax.ppermute(value, 'sp', [(s, s + group) for s in range(n_sp - group)])  11.6 us
    dot_general x5, matrix products, local(): lowered = jnp.dot(hidden, downs[index], preferred_element_type=jnp.float32)  11.4 us
  transfers between devices with their start and end apart: 52, of which 22 were waited for; matrix products, arithmetic and copies ran while one was open for 10% of the time, Pallas kernels for 14%

profile of v1, /device:TPU:0, one launch (start us, length us, event | category | flops | bytes accessed | tf_op | source)
XLA Modules:
  0.0 318.6 jit_solution(4378042490230396155)
XLA Ops:
  14.3 10.4 %collective-permute-done.11.refs_13_ = f32[2,17,384]{2,1,0:T(8,128)S(1)} collective-permute-done((f32[2,17,384]{2,1,0:T(8,128)S(1)}, f32[2,17,384]{2,1,0:T(8,128)S(1)}, u32[]{:S(2)}, u32[]{:S(2)}) %collective-permute-start.11) | collective-permute-done | bytes 52256 | tf_op jit(solution)/shard_map/ppermute | solution.py:344
  36.6 3.5 %collective-permute-start.6 = (bf16[384,512]{1,0:T(8,128)(2,1)S(1)}, bf16[384,512]{1,0:T(8,128)(2,1)S(1)}, u32[]{:S(2)}, u32[]{:S(2)}) collective-permute-start(bf16[384,512]{1,0:T(8,128)(2,1)S(1)} %pad_maximum_fusion.3.refs_4_), channel_id=1, source_target_pairs={{0,8},{2,10},{4,12},{6,14},{8,16},{10,18},{12,20},{14,22},{16,24},... | collective-permute-start | bytes 1179656 | tf_op jit(solution)/shard_map/ppermute | solution.py:347
  40.1 3.5 %collective-permute-start.7 = (bf16[384,512]{1,0:T(8,128)(2,1)}, bf16[384,512]{1,0:T(8,128)(2,1)S(1)}, u32[]{:S(2)}, u32[]{:S(2)}) collective-permute-start(bf16[384,512]{1,0:T(8,128)(2,1)} %collective-permute-done.3.refs_5_), channel_id=1, source_target_pairs={{0,8},{2,10},{4,12},{6,14},{8,16},{10,18},{12,20},{14,22},{16,24},... | collective-permute-start | bytes 1179656 | tf_op jit(solution)/shard_map/ppermute | solution.py:347
  52.1 4.4 %collective-permute-done.2.refs_3_ = bf16[384,256]{1,0:T(8,128)(2,1)S(1)} collective-permute-done((bf16[384,256]{1,0:T(8,128)(2,1)S(1)}, bf16[384,256]{1,0:T(8,128)(2,1)S(1)}, u32[]{:S(2)}, u32[]{:S(2)}) %collective-permute-start.2) | collective-permute-done | bytes 196640 | tf_op jit(solution)/shard_map/ppermute | solution.py:344
  58.1 4.4 %collective-permute-start.30 = (bf16[128,1280]{1,0:T(8,128)(2,1)}, bf16[128,1280]{1,0:T(8,128)(2,1)S(1)}, u32[]{:S(2)}, u32[]{:S(2)}) collective-permute-start(bf16[128,1280]{1,0:T(8,128)(2,1)} %get-tuple-element.38), channel_id=1, source_target_pairs={{0,24},{2,26},{4,28},{6,30},{8,16},{10,18},{12,20},{14,22},{16,8},... | collective-permute-start | bytes 983048 | tf_op jit(solution)/shard_map/ppermute | solution.py:344
  62.5 4.0 %collective-permute-done.8.refs_10_ = bf16[384,512]{1,0:T(8,128)(2,1)S(1)} collective-permute-done((bf16[384,512]{1,0:T(8,128)(2,1)}, bf16[384,512]{1,0:T(8,128)(2,1)S(1)}, u32[]{:S(2)}, u32[]{:S(2)}) %collective-permute-start.8) | collective-permute-done | bytes 393248 | tf_op jit(solution)/shard_map/ppermute | solution.py:347
  69.8 5.1 %collective-permute-done.9.refs_11_ = bf16[384,512]{1,0:T(8,128)(2,1)S(1)} collective-permute-done((bf16[384,512]{1,0:T(8,128)(2,1)}, bf16[384,512]{1,0:T(8,128)(2,1)S(1)}, u32[]{:S(2)}, u32[]{:S(2)}) %collective-permute-start.9) | collective-permute-done | bytes 393248 | tf_op jit(solution)/shard_map/ppermute | solution.py:347
  74.9 14.0 %collective-permute-start.22 = (bf16[128,1280]{1,0:T(8,128)(2,1)S(1)}, bf16[128,1280]{1,0:T(8,128)(2,1)S(1)}, u32[]{:S(2)}, u32[]{:S(2)}) collective-permute-start(bf16[128,1280]{1,0:T(8,128)(2,1)S(1)} %get-tuple-element.39), channel_id=1, source_target_pairs={{0,16},{2,18},{4,20},{6,22},{8,24},{10,26},{12,28},{14,30},{16,0},... | collective-permute-start | bytes 983048 | tf_op jit(solution)/shard_map/ppermute | solution.py:344
  88.9 23.7 %attend.1 = (bf16[384,256]{1,0:T(8,128)(2,1)}, bf16[384,256]{1,0:T(8,128)(2,1)}, bf16[384,256]{1,0:T(8,128)(2,1)}, bf16[384,256]{1,0:T(8,128)(2,1)}) custom-call(s32[1]{0:T(128)} %bitcast.2.where_ref, bf16[384,256]{1,0:T(8,128)(2,1)} %get-tuple-element.33.refs_0_, bf16[384,256]{1,0:T(8,128)(2,1)} %collective-permute-done.refs_1_, ...), custom_call_target="tpu_custom_call" | custom-call | flops 9663676416 | bytes 6291456 | tf_op jit(solution)/shard_map/attend/pallas_call | solution.py:112
  117.5 4.1 %collective-permute-done.14.refs_1_ = bf16[384,256]{1,0:T(8,128)(2,1)S(1)} collective-permute-done((bf16[384,256]{1,0:T(8,128)(2,1)}, bf16[384,256]{1,0:T(8,128)(2,1)S(1)}, u32[]{:S(2)}, u32[]{:S(2)}) %collective-permute-start.14) | collective-permute-done | bytes 196640 | tf_op jit(solution)/shard_map/ppermute | solution.py:344
  125.1 16.2 %collective-permute-done.16.refs_3_ = bf16[384,256]{1,0:T(8,128)(2,1)S(1)} collective-permute-done((bf16[384,256]{1,0:T(8,128)(2,1)S(1)}, bf16[384,256]{1,0:T(8,128)(2,1)S(1)}, u32[]{:S(2)}, u32[]{:S(2)}) %collective-permute-start.16) | collective-permute-done | bytes 196640 | tf_op jit(solution)/shard_map/ppermute | solution.py:344
  141.2 14.9 %collective-permute-start.37 = (bf16[1280,128]{1,0:T(8,128)(2,1)}, bf16[1280,128]{1,0:T(8,128)(2,1)}, u32[]{:S(2)}, u32[]{:S(2)}) collective-permute-start(bf16[1280,128]{1,0:T(8,128)(2,1)} %get-tuple-element.36), channel_id=1, source_target_pairs={{0,24},{2,26},{4,28},{6,30},{8,16},{10,18},{12,20},{14,22},{16,8},... | collective-permute-start | bytes 983048 | tf_op jit(solution)/shard_map/ppermute | solution.py:344
  156.2 5.3 %project.1 = (bf16[192,2048]{1,0:T(8,128)(2,1)}, bf16[192,2048]{1,0:T(8,128)(2,1)}) custom-call(s32[2]{0:T(128)} %pad_add_fusion.1.where_ref, bf16[384,256]{1,0:T(8,128)(2,1)} %get-tuple-element.14.refs_0_, bf16[384,256]{1,0:T(8,128)(2,1)} %copy-done.37, bf16[384,256]{1,0:T(8,128)(2,1)} %copy-done.38, bf16[384,256]{1,0:T(8,128)(2,1)} %copy-done.39, ...), custom_call_target="tpu_custom_call" | custom-call | flops 1610612736 | bytes 4194304 | tf_op jit(solution)/shard_map/project/pallas_call | solution.py:158
  166.8 4.2 %collective-permute-done.36 = bf16[1280,128]{1,0:T(8,128)(2,1)S(1)} collective-permute-done((bf16[1280,128]{1,0:T(8,128)(2,1)S(1)}, bf16[1280,128]{1,0:T(8,128)(2,1)S(1)}, u32[]{:S(2)}, u32[]{:S(2)}) %collective-permute-start.36) | collective-permute-done | bytes 327712 | tf_op jit(solution)/shard_map/ppermute | solution.py:344
  170.9 7.3 %collective-permute-done.35 = bf16[1280,128]{1,0:T(8,128)(2,1)S(1)} collective-permute-done((bf16[1280,128]{1,0:T(8,128)(2,1)}, bf16[1280,128]{1,0:T(8,128)(2,1)S(1)}, u32[]{:S(2)}, u32[]{:S(2)}) %collective-permute-start.35) | collective-permute-done | bytes 327712 | tf_op jit(solution)/shard_map/ppermute | solution.py:344
  184.5 3.8 %middle.1 = (bf16[192,2048]{1,0:T(8,128)(2,1)}, bf16[192,2048]{1,0:T(8,128)(2,1)}, bf16[192,2048]{1,0:T(8,128)(2,1)}) custom-call(s32[2]{0:T(128)} %pad_add_fusion.where_ref, bf16[384,2048]{1,0:T(8,128)(2,1)} %residual_ref.1, bf16[192,2048]{1,0:T(8,128)(2,1)} %get-tuple-element.18.refs_0_, bf16[192,2048]{1,0:T(8,128)(2,1)} %collective-permute-done.17.refs_1_, ...), custom_call_target="tpu_custom_call" | custom-call | flops 786432000 | bytes 3932160 | tf_op jit(solution)/shard_map/middle/pallas_call | solution.py:207
  189.5 7.5 %collective-permute-done.31.refs_10_ = bf16[512,1280]{1,0:T(8,128)(2,1)} collective-permute-done((bf16[512,1280]{1,0:T(8,128)(2,1)S(1)}, bf16[512,1280]{1,0:T(8,128)(2,1)}, u32[]{:S(2)}, u32[]{:S(2)}) %collective-permute-start.31) | collective-permute-done | bytes 1310752 | tf_op jit(solution)/shard_map/ppermute | solution.py:344
  198.5 11.4 %collective-permute-done.32.refs_11_ = bf16[512,1280]{1,0:T(8,128)(2,1)} collective-permute-done((bf16[512,1280]{1,0:T(8,128)(2,1)S(1)}, bf16[512,1280]{1,0:T(8,128)(2,1)}, u32[]{:S(2)}, u32[]{:S(2)}) %collective-permute-start.32) | collective-permute-done | bytes 1310752 | tf_op jit(solution)/shard_map/ppermute | solution.py:344
  213.9 11.3 %collective-permute-done.39 = bf16[1280,512]{1,0:T(8,128)(2,1)} collective-permute-done((bf16[1280,512]{1,0:T(8,128)(2,1)}, bf16[1280,512]{1,0:T(8,128)(2,1)}, u32[]{:S(2)}, u32[]{:S(2)}) %collective-permute-start.39) | collective-permute-done | bytes 1310752 | tf_op jit(solution)/shard_map/ppermute | solution.py:344
  225.7 12.4 %collective-permute-done.41 = bf16[1280,512]{1,0:T(8,128)(2,1)} collective-permute-done((bf16[1280,512]{1,0:T(8,128)(2,1)}, bf16[1280,512]{1,0:T(8,128)(2,1)}, u32[]{:S(2)}, u32[]{:S(2)}) %collective-permute-start.41) | collective-permute-done | bytes 1310752 | tf_op jit(solution)/shard_map/ppermute | solution.py:344
  244.2 7.8 %collective-permute-done.27.refs_8_ = bf16[256,1280]{1,0:T(8,128)(2,1)S(1)} collective-permute-done((bf16[256,1280]{1,0:T(8,128)(2,1)S(1)}, bf16[256,1280]{1,0:T(8,128)(2,1)S(1)}, u32[]{:S(2)}, u32[]{:S(2)}) %collective-permute-start.27) | collective-permute-done | bytes 655392 | tf_op jit(solution)/shard_map/ppermute | solution.py:344
  255.6 10.5 %collective-permute-done.34.refs_13_ = bf16[256,1280]{1,0:T(8,128)(2,1)S(1)} collective-permute-done((bf16[256,1280]{1,0:T(8,128)(2,1)S(1)}, bf16[256,1280]{1,0:T(8,128)(2,1)S(1)}, u32[]{:S(2)}, u32[]{:S(2)}) %collective-permute-start.34) | collective-permute-done | bytes 655392 | tf_op jit(solution)/shard_map/ppermute | solution.py:344
  267.8 13.2 %mix.1 = bf16[768,1280]{1,0:T(8,128)(2,1)} custom-call(bf16[192,2048]{1,0:T(8,128)(2,1)} %get-tuple-element.21.refs_0_, bf16[192,2048]{1,0:T(8,128)(2,1)} %copy-done.25, bf16[192,2048]{1,0:T(8,128)(2,1)} %copy-done.24, bf16[192,2048]{1,0:T(8,128)(2,1)} %collective-permute-done.20.refs_3_, bf16[512,1280]{1,0:T(8,128)(2,1)} %copy-done, ...), custom_call_target="tpu_custom_call" | custom-call | flops 8053063680 | bytes 15597568 | tf_op jit(solution)/shard_map/mix/pallas_call | solution.py:265
  307.4 4.2 %collective-permute-done.48.refs_6_ = bf16[192,512]{1,0:T(8,128)(2,1)S(1)} collective-permute-done((bf16[192,512]{1,0:T(8,128)(2,1)S(1)}, bf16[192,512]{1,0:T(8,128)(2,1)S(1)}, u32[]{:S(2)}, u32[]{:S(2)}) %collective-permute-start.48) | collective-permute-done | bytes 196640 | tf_op jit(solution)/shard_map/ppermute | solution.py:344
  (220 shorter events, 111.0 us)
Async XLA Ops:
  1.7 38.4 %collective-permute-start.3 = (bf16[384,512]{1,0:T(8,128)(2,1)S(1)}, bf16[384,512]{1,0:T(8,128)(2,1)}, u32[]{:S(2)}, u32[]{:S(2)}) collective-permute-start(bf16[384,512]{1,0:T(8,128)(2,1)S(1)} %pad_maximum_fusion.4), channel_id=1, source_target_pairs={{0,2},{2,0},{4,6},{6,4},{8,10},{10,8},{12,14},{14,12},{16,18},{18,... | collective-permute-start | bytes 1179656 | tf_op jit(solution)/shard_map/ppermute | solution.py:344
  4.7 38.9 %collective-permute-start.4 = (bf16[384,512]{1,0:T(8,128)(2,1)S(1)}, bf16[384,512]{1,0:T(8,128)(2,1)}, u32[]{:S(2)}, u32[]{:S(2)}) collective-permute-start(bf16[384,512]{1,0:T(8,128)(2,1)S(1)} %pad_maximum_fusion.5), channel_id=1, source_target_pairs={{0,4},{2,6},{4,0},{6,2},{8,12},{10,14},{12,8},{14,10},{16,20},{18,... | collective-permute-start | bytes 1179656 | tf_op jit(solution)/shard_map/ppermute | solution.py:344
  9.9 37.2 %collective-permute-start.5 = (bf16[384,512]{1,0:T(8,128)(2,1)S(1)}, bf16[384,512]{1,0:T(8,128)(2,1)}, u32[]{:S(2)}, u32[]{:S(2)}) collective-permute-start(bf16[384,512]{1,0:T(8,128)(2,1)S(1)} %pad_maximum_fusion.6), channel_id=1, source_target_pairs={{0,6},{2,4},{4,2},{6,0},{8,14},{10,12},{12,10},{14,8},{16,22},{18,... | collective-permute-start | bytes 1179656 | tf_op jit(solution)/shard_map/ppermute | solution.py:344
  47.1 27.8 %collective-permute-start.9 = (bf16[384,512]{1,0:T(8,128)(2,1)}, bf16[384,512]{1,0:T(8,128)(2,1)S(1)}, u32[]{:S(2)}, u32[]{:S(2)}) collective-permute-start(bf16[384,512]{1,0:T(8,128)(2,1)} %collective-permute-done.5.refs_7_), channel_id=1, source_target_pairs={{0,8},{2,10},{4,12},{6,14},{8,16},{10,18},{12,20},{14,22},{16,24},... | collective-permute-start | bytes 1179656 | tf_op jit(solution)/shard_map/ppermute | solution.py:347
  56.5 56.2 %collective-permute-start.23 = (bf16[128,1280]{1,0:T(8,128)(2,1)}, bf16[128,1280]{1,0:T(8,128)(2,1)S(1)}, u32[]{:S(2)}, u32[]{:S(2)}) collective-permute-start(bf16[128,1280]{1,0:T(8,128)(2,1)} %get-tuple-element.40), channel_id=1, source_target_pairs={{0,24},{2,26},{4,28},{6,30},{8,16},{10,18},{12,20},{14,22},{16,8},... | collective-permute-start | bytes 983048 | tf_op jit(solution)/shard_map/ppermute | solution.py:344
  56.5 58.6 %collective-permute-start.21 = (bf16[128,1280]{1,0:T(8,128)(2,1)}, bf16[128,1280]{1,0:T(8,128)(2,1)S(1)}, u32[]{:S(2)}, u32[]{:S(2)}) collective-permute-start(bf16[128,1280]{1,0:T(8,128)(2,1)} %get-tuple-element.40), channel_id=1, source_target_pairs={{0,8},{2,10},{4,12},{6,14},{8,0},{10,2},{12,4},{14,6},{16,24},{18,... | collective-permute-start | bytes 983048 | tf_op jit(solution)/shard_map/ppermute | solution.py:344
  58.1 103.5 %collective-permute-start.30 = (bf16[128,1280]{1,0:T(8,128)(2,1)}, bf16[128,1280]{1,0:T(8,128)(2,1)S(1)}, u32[]{:S(2)}, u32[]{:S(2)}) collective-permute-start(bf16[128,1280]{1,0:T(8,128)(2,1)} %get-tuple-element.38), channel_id=1, source_target_pairs={{0,24},{2,26},{4,28},{6,30},{8,16},{10,18},{12,20},{14,22},{16,8},... | collective-permute-start | bytes 983048 | tf_op jit(solution)/shard_map/ppermute | solution.py:344
  66.5 96.7 %collective-permute-start.28 = (bf16[128,1280]{1,0:T(8,128)(2,1)}, bf16[128,1280]{1,0:T(8,128)(2,1)S(1)}, u32[]{:S(2)}, u32[]{:S(2)}) collective-permute-start(bf16[128,1280]{1,0:T(8,128)(2,1)} %get-tuple-element.38), channel_id=1, source_target_pairs={{0,8},{2,10},{4,12},{6,14},{8,0},{10,2},{12,4},{14,6},{16,24},{18,... | collective-permute-start | bytes 983048 | tf_op jit(solution)/shard_map/ppermute | solution.py:344
  74.9 38.7 %collective-permute-start.22 = (bf16[128,1280]{1,0:T(8,128)(2,1)S(1)}, bf16[128,1280]{1,0:T(8,128)(2,1)S(1)}, u32[]{:S(2)}, u32[]{:S(2)}) collective-permute-start(bf16[128,1280]{1,0:T(8,128)(2,1)S(1)} %get-tuple-element.39), channel_id=1, source_target_pairs={{0,16},{2,18},{4,20},{6,22},{8,24},{10,26},{12,28},{14,30},{16,0},... | collective-permute-start | bytes 983048 | tf_op jit(solution)/shard_map/ppermute | solution.py:344
  112.7 48.9 %collective-permute-start.29 = (bf16[128,1280]{1,0:T(8,128)(2,1)S(1)}, bf16[128,1280]{1,0:T(8,128)(2,1)S(1)}, u32[]{:S(2)}, u32[]{:S(2)}) collective-permute-start(bf16[128,1280]{1,0:T(8,128)(2,1)S(1)} %get-tuple-element.37), channel_id=1, source_target_pairs={{0,16},{2,18},{4,20},{6,22},{8,24},{10,26},{12,28},{14,30},{16,0},... | collective-permute-start | bytes 983048 | tf_op jit(solution)/shard_map/ppermute | solution.py:344
  121.6 60.3 %collective-permute-start.24 = (bf16[512,1280]{1,0:T(8,128)(2,1)S(1)}, bf16[512,1280]{1,0:T(8,128)(2,1)}, u32[]{:S(2)}, u32[]{:S(2)}) collective-permute-start(bf16[512,1280]{1,0:T(8,128)(2,1)S(1)} %pad_maximum_fusion.refs_4_), channel_id=1, source_target_pairs={{0,2},{2,0},{4,6},{6,4},{8,10},{10,8},{12,14},{14,12},{16,18},{18,... | collective-permute-start | bytes 3932168 | tf_op jit(solution)/shard_map/ppermute | solution.py:344
  141.2 24.0 %collective-permute-start.37 = (bf16[1280,128]{1,0:T(8,128)(2,1)}, bf16[1280,128]{1,0:T(8,128)(2,1)}, u32[]{:S(2)}, u32[]{:S(2)}) collective-permute-start(bf16[1280,128]{1,0:T(8,128)(2,1)} %get-tuple-element.36), channel_id=1, source_target_pairs={{0,24},{2,26},{4,28},{6,30},{8,16},{10,18},{12,20},{14,22},{16,8},... | collective-permute-start | bytes 983048 | tf_op jit(solution)/shard_map/ppermute | solution.py:344
  161.6 26.7 %collective-permute-start.25 = (bf16[512,1280]{1,0:T(8,128)(2,1)S(1)}, bf16[512,1280]{1,0:T(8,128)(2,1)}, u32[]{:S(2)}, u32[]{:S(2)}) collective-permute-start(bf16[512,1280]{1,0:T(8,128)(2,1)S(1)} %pad_maximum_fusion.refs_4_), channel_id=1, source_target_pairs={{0,4},{2,6},{4,0},{6,2},{8,12},{10,14},{12,8},{14,10},{16,20},{18,... | collective-permute-start | bytes 3932168 | tf_op jit(solution)/shard_map/ppermute | solution.py:344
  165.3 31.8 %collective-permute-start.31 = (bf16[512,1280]{1,0:T(8,128)(2,1)S(1)}, bf16[512,1280]{1,0:T(8,128)(2,1)}, u32[]{:S(2)}, u32[]{:S(2)}) collective-permute-start(bf16[512,1280]{1,0:T(8,128)(2,1)S(1)} %pad_maximum_fusion.1.refs_9_), channel_id=1, source_target_pairs={{0,2},{2,0},{4,6},{6,4},{8,10},{10,8},{12,14},{14,12},{16,18},{18,... | collective-permute-start | bytes 3932168 | tf_op jit(solution)/shard_map/ppermute | solution.py:344
  178.2 31.8 %collective-permute-start.32 = (bf16[512,1280]{1,0:T(8,128)(2,1)S(1)}, bf16[512,1280]{1,0:T(8,128)(2,1)}, u32[]{:S(2)}, u32[]{:S(2)}) collective-permute-start(bf16[512,1280]{1,0:T(8,128)(2,1)S(1)} %pad_maximum_fusion.1.refs_9_), channel_id=1, source_target_pairs={{0,4},{2,6},{4,0},{6,2},{8,12},{10,14},{12,8},{14,10},{16,20},{18,... | collective-permute-start | bytes 3932168 | tf_op jit(solution)/shard_map/ppermute | solution.py:344
  181.9 43.3 %collective-permute-start.39 = (bf16[1280,512]{1,0:T(8,128)(2,1)}, bf16[1280,512]{1,0:T(8,128)(2,1)}, u32[]{:S(2)}, u32[]{:S(2)}) collective-permute-start(bf16[1280,512]{1,0:T(8,128)(2,1)} %pad_maximum_fusion.2), channel_id=1, source_target_pairs={{0,2},{2,0},{4,6},{6,4},{8,10},{10,8},{12,14},{14,12},{16,18},{18,... | collective-permute-start | bytes 3932168 | tf_op jit(solution)/shard_map/ppermute | solution.py:344
  183.4 54.7 %collective-permute-start.41 = (bf16[1280,512]{1,0:T(8,128)(2,1)}, bf16[1280,512]{1,0:T(8,128)(2,1)}, u32[]{:S(2)}, u32[]{:S(2)}) collective-permute-start(bf16[1280,512]{1,0:T(8,128)(2,1)} %pad_maximum_fusion.2), channel_id=1, source_target_pairs={{0,4},{2,6},{4,0},{6,2},{8,12},{10,14},{12,8},{14,10},{16,20},{18,... | collective-permute-start | bytes 3932168 | tf_op jit(solution)/shard_map/ppermute | solution.py:344
  197.1 42.5 %collective-permute-start.26 = (bf16[256,1280]{1,0:T(8,128)(2,1)S(1)}, bf16[256,1280]{1,0:T(8,128)(2,1)S(1)}, u32[]{:S(2)}, u32[]{:S(2)}) collective-permute-start(bf16[256,1280]{1,0:T(8,128)(2,1)S(1)} %slice.114), channel_id=1, source_target_pairs={{0,2},{2,0},{4,6},{6,4},{8,10},{10,8},{12,14},{14,12},{16,18},{18,... | collective-permute-start | bytes 1966088 | tf_op jit(solution)/shard_map/ppermute | solution.py:344
  210.0 56.1 %collective-permute-start.18 = (bf16[192,2048]{1,0:T(8,128)(2,1)}, bf16[192,2048]{1,0:T(8,128)(2,1)S(1)}, u32[]{:S(2)}, u32[]{:S(2)}) collective-permute-start(bf16[192,2048]{1,0:T(8,128)(2,1)} %get-tuple-element.21.refs_0_), channel_id=1, source_target_pairs={{0,1},{1,0},{2,3},{3,2},{4,5},{5,4},{6,7},{7,6},{8,9},{9,8},{10,11... | collective-permute-start | bytes 2359304 | tf_op jit(solution)/shard_map/ppermute | solution.py:350
  210.0 56.9 %collective-permute-start.20 = (bf16[192,2048]{1,0:T(8,128)(2,1)S(1)}, bf16[192,2048]{1,0:T(8,128)(2,1)}, u32[]{:S(2)}, u32[]{:S(2)}) collective-permute-start(bf16[192,2048]{1,0:T(8,128)(2,1)S(1)} %collective-permute-done.19.refs_2_), channel_id=1, source_target_pairs={{0,1},{1,0},{2,3},{3,2},{4,5},{5,4},{6,7},{7,6},{8,9},{9,8},{10,11... | collective-permute-start | bytes 2359304 | tf_op jit(solution)/shard_map/ppermute | solution.py:350
  225.2 26.8 %collective-permute-start.27 = (bf16[256,1280]{1,0:T(8,128)(2,1)S(1)}, bf16[256,1280]{1,0:T(8,128)(2,1)S(1)}, u32[]{:S(2)}, u32[]{:S(2)}) collective-permute-start(bf16[256,1280]{1,0:T(8,128)(2,1)S(1)} %slice.115), channel_id=1, source_target_pairs={{0,4},{2,6},{4,0},{6,2},{8,12},{10,14},{12,8},{14,10},{16,20},{18,... | collective-permute-start | bytes 1966088 | tf_op jit(solution)/shard_map/ppermute | solution.py:344
  240.4 25.7 %collective-permute-start.34 = (bf16[256,1280]{1,0:T(8,128)(2,1)S(1)}, bf16[256,1280]{1,0:T(8,128)(2,1)S(1)}, u32[]{:S(2)}, u32[]{:S(2)}) collective-permute-start(bf16[256,1280]{1,0:T(8,128)(2,1)S(1)} %slice.117), channel_id=1, source_target_pairs={{0,4},{2,6},{4,0},{6,2},{8,12},{10,14},{12,8},{14,10},{16,20},{18,... | collective-permute-start | bytes 1966088 | tf_op jit(solution)/shard_map/ppermute | solution.py:344
  252.0 37.7 %collective-permute-start.43 = (bf16[1280,256]{1,0:T(8,128)(2,1)S(1)}, bf16[1280,256]{1,0:T(8,128)(2,1)}, u32[]{:S(2)}, u32[]{:S(2)}) collective-permute-start(bf16[1280,256]{1,0:T(8,128)(2,1)S(1)} %slice.127), channel_id=1, source_target_pairs={{0,2},{2,0},{4,6},{6,4},{8,10},{10,8},{12,14},{14,12},{16,18},{18,... | collective-permute-start | bytes 1966088 | tf_op jit(solution)/shard_map/ppermute | solution.py:344
  255.6 36.5 %collective-permute-start.45 = (bf16[1280,256]{1,0:T(8,128)(2,1)S(1)}, bf16[1280,256]{1,0:T(8,128)(2,1)}, u32[]{:S(2)}, u32[]{:S(2)}) collective-permute-start(bf16[1280,256]{1,0:T(8,128)(2,1)S(1)} %slice.131), channel_id=1, source_target_pairs={{0,4},{2,6},{4,0},{6,2},{8,12},{10,14},{12,8},{14,10},{16,20},{18,... | collective-permute-start | bytes 1966088 | tf_op jit(solution)/shard_map/ppermute | solution.py:344
  (71 other events, 960.8 us)
